TPU v7x, 256 devices: a 2x2x32 block of a 4x8x32 slice. The times are simulated.
256 devices in a mesh: grp: 4 (over y, x), ep: 64 (over z, core).
Axes of the slice: x: 2, y: 2, z: 32, core: 2. Of those that a mesh axis runs over, the one named last changes fastest.
The devices are a block of a 4x8x32 slice.
Arguments:
- tokens: bfloat16 [65536, 2048], P(('grp', 'ep')), parts along dimension 0, may hold values from -6 to 6
- norm_gain: float32 [2048], replicated, may hold values from 0.1 to 1.9
- routes: int32 [65536, 2], P(('grp', 'ep')), parts along dimension 0, may hold values from 0 to 63, all different within a row; in each aligned block of 256 rows (0 to 255, 256 to 511, ...) at most 10 rows name the same one
- route_weights: float32 [65536, 2], P(('grp', 'ep')), parts along dimension 0, may hold values from 0.2 to 1.5
- expert_gate: bfloat16 [64, 2048, 256], P('ep'), may hold values from -0.125 to 0.125
- expert_up: bfloat16 [64, 2048, 256], P('ep'), may hold values from -0.125 to 0.125
- expert_down: bfloat16 [64, 256, 2048], P('ep'), may hold values from -0.375 to 0.375
- shared_gate: bfloat16 [2048, 256], replicated, may hold values from -0.125 to 0.125
- shared_up: bfloat16 [2048, 256], replicated, may hold values from -0.125 to 0.125
- shared_down: bfloat16 [256, 2048], replicated, may hold values from -0.375 to 0.375
Outputs:
- mixed: bfloat16 [65536, 2048], P(('grp', 'ep')), parts along dimension 0
There are 4 independent parts, one for each index of `grp`. A program takes and returns all parts, laid end to end along the dimension named above; an argument that names none is the same for every part. Nothing has to cross between parts.
Inputs may be any that keep to these rules, and one draw needn't show every extreme that they name: `routes`: the 2 experts of a token are distinct. Among the tokens of one device, at most 10 choose any one expert; in every draw some expert is chosen by exactly 10 tokens of some device.
All inputs are finite; a program needn't handle non-finite values.
Results may differ from a plain program's by a relative error of at most 0.0075.
Values may be sent and summed in bfloat16 or wider, within the bound.
No kernel may reach another device: no remote copies, remote signals or barrier semaphores. Data moves between devices by JAX's collectives and lax.ppermute only.
A program may use at most 64 MiB of HBM per device.

v0:
```python
import jax
import jax.numpy as jnp
from jax import lax
from jax.sharding import PartitionSpec as P


def swiglu_rows(row_block, w_gate, w_up, w_down):
    gate_part = jnp.dot(row_block, w_gate, preferred_element_type=jnp.float32)
    up_part = jnp.dot(row_block, w_up, preferred_element_type=jnp.float32)
    hidden = (jax.nn.silu(gate_part) * up_part).astype(jnp.bfloat16)
    return jnp.dot(hidden, w_down, preferred_element_type=jnp.float32)


def on_device(
    tokens,
    norm_gain,
    routes,
    route_weights,
    expert_gate,
    expert_up,
    expert_down,
    shared_gate,
    shared_up,
    shared_down,
):
    tok_rows, model_width = tokens.shape
    top_count = routes.shape[1]
    devices_ep = lax.axis_size("ep")
    capacity = 5 * tok_rows * top_count // (4 * devices_ep)
    upcast = tokens.astype(jnp.float32)
    factor = lax.rsqrt(jnp.mean(upcast * upcast, axis=-1, keepdims=True) + 1e-06)
    normed = (upcast * factor * norm_gain).astype(jnp.bfloat16)
    flat_expert = routes.reshape(-1)
    onehot = (flat_expert[:, None] == jnp.arange(devices_ep, dtype=jnp.int32)[None, :]).astype(
        jnp.int32
    )
    position = jnp.sum(jnp.cumsum(onehot, axis=0) * onehot, axis=1) - 1
    slot_index = flat_expert * capacity + position
    pair_token = jnp.arange(tok_rows * top_count, dtype=jnp.int32) // top_count
    slot_token = (
        jnp.full((devices_ep * capacity,), tok_rows, jnp.int32).at[slot_index].set(pair_token)
    )
    padded = jnp.concatenate([normed, jnp.zeros((1, model_width), jnp.bfloat16)], axis=0)
    outgoing = padded[slot_token].reshape(devices_ep, capacity, model_width)
    arrived = lax.all_to_all(outgoing, "ep", split_axis=0, concat_axis=0, tiled=True)
    flat_rows = arrived.reshape(devices_ep * capacity, model_width)
    expert_rows = swiglu_rows(flat_rows, expert_gate[0], expert_up[0], expert_down[0]).astype(
        jnp.bfloat16
    )
    returned = lax.all_to_all(
        expert_rows.reshape(devices_ep, capacity, model_width),
        "ep",
        split_axis=0,
        concat_axis=0,
        tiled=True,
    )
    pair_out = returned.reshape(devices_ep * capacity, model_width)[slot_index]
    pair_out = pair_out.reshape(tok_rows, top_count, model_width)
    routed = jnp.einsum("tk,tkd->td", route_weights, pair_out.astype(jnp.float32))
    shared_result = swiglu_rows(normed, shared_gate, shared_up, shared_down)
    return (routed + shared_result).astype(jnp.bfloat16)


def solution(mesh):
    return jax.shard_map(
        on_device,
        mesh=mesh,
        in_specs=(
            P(("grp", "ep"), None),
            P(),
            P(("grp", "ep"), None),
            P(("grp", "ep"), None),
            P("ep", None, None),
            P("ep", None, None),
            P("ep", None, None),
            P(),
            P(),
            P(),
        ),
        out_specs=P(("grp", "ep"), None),
        check_vma=False,
    )
```

profile of v0, /device:TPU:37, one launch (start us, length us, event | category | flops | bytes accessed | tf_op | source)
XLA Modules:
  0.0 865.0 jit_solution(12289669756593723275)
XLA Ops:
  0.0 0.0 copy-start
  0.0 0.0 copy-start.1
  0.0 0.0 copy-start.4
  0.0 1.0 copy.12
  1.0 0.1 eq.29
  1.1 0.1 eq.25
  1.3 0.7 broadcast_multiply_fusion
  2.0 1.2 reduce-window.6
  3.2 0.2 slice_reduce_fusion
  3.5 0.1 fusion.23
  3.6 0.1 copy.11
  3.7 0.1 mul.59
  3.9 2.4 scatter_custom_fusion
  6.4 0.0 copy-done.1
  6.4 0.3 fusion.1
  6.7 0.0 copy-done.4
  6.7 0.3 fusion.3
  7.0 0.1 concatenate.3
  7.1 4.1 gather_fusion
  11.2 5.4 reshape.76
  16.6 411.6 %all_to_all.10 = bf16[64,10,2048]{2,1,0:T(8,128)(2,1)} all-to-all(bf16[64,10,2048]{2,1,0:T(8,128)(2,1)} %reshape.76), channel_id=1, replica_groups=mesh['grp'=4,'ep'=64] {'ep'}, dimensions={0} | all-to-all | bytes 5242880 | tf_op jit(solution)/shard_map/all_to_all | solution.py:45
  428.1 0.0 copy-start.6
  428.1 5.6 reshape.77
  433.8 0.0 copy-done.6
  433.8 3.4 fusion.9
  437.2 0.0 copy-done
  437.2 6.6 convolution_convert_fusion
  443.8 5.4 reshape.78
  449.1 0.0 copy-start.5
  449.2 0.0 copy-start.3
  449.2 8.8 %all-to-all-start.1 = ((bf16[64,10,2048]{2,1,0:T(8,128)(2,1)}), bf16[64,10,2048]{2,1,0:T(8,128)(2,1)}, u32[]{:S(2)}, u32[]{:S(2)}) async-start(bf16[64,10,2048]{2,1,0:T(8,128)(2,1)} %reshape.78), calls=%async_computation.1 | async-start | bytes 8388608 | tf_op jit(solution)/shard_map/all_to_all | solution.py:50
  457.9 0.0 copy-done.5
  457.9 0.2 copy.15
  458.1 0.0 copy-done.3
  458.1 0.4 fusion.34
  458.6 379.4 %all-to-all-done.1 = bf16[64,10,2048]{2,1,0:T(8,128)(2,1)} async-done(((bf16[64,10,2048]{2,1,0:T(8,128)(2,1)}), bf16[64,10,2048]{2,1,0:T(8,128)(2,1)}, u32[]{:S(2)}, u32[]{:S(2)}) %all-to-all-start.1) | async-done | bytes 2621472 | tf_op jit(solution)/shard_map/all_to_all | solution.py:50
  838.0 5.5 reshape.79
  843.6 7.4 gather_fusion.1
  850.9 4.4 reshape.80
  855.3 0.0 copy-start.2
  855.3 5.3 fusion.33
  860.7 0.0 copy-done.2
  860.7 4.4 fusion
  (10 shorter events, 0.1 us)
Async XLA Ops:
  0.0 437.2 %copy-start = (bf16[1,256,2048]{2,1,0:T(8,128)(2,1)S(1)}, bf16[1,256,2048]{2,1,0:T(8,128)(2,1)}, u32[]{:S(2)}) copy-start(bf16[1,256,2048]{2,1,0:T(8,128)(2,1)} %param.16) | copy-start | bytes 3145732
  0.0 6.4 copy-start.1
  0.0 6.7 copy-start.4
  428.1 5.6 copy-start.6
  449.1 8.8 %copy-start.5 = (f32[256,2]{0,1:T(2,128)S(1)}, f32[256,2]{0,1:T(2,128)}, u32[]{:S(2)}) copy-start(f32[256,2]{0,1:T(2,128)} %param.13) | copy-start | bytes 6148
  449.2 9.0 %copy-start.3 = (bf16[2048,256]{1,0:T(8,128)(2,1)S(1)}, bf16[2048,256]{1,0:T(8,128)(2,1)}, u32[]{:S(2)}) copy-start(bf16[2048,256]{1,0:T(8,128)(2,1)} %param.17) | copy-start | bytes 3145732
  449.2 388.9 %all-to-all-start.1 = ((bf16[64,10,2048]{2,1,0:T(8,128)(2,1)}), bf16[64,10,2048]{2,1,0:T(8,128)(2,1)}, u32[]{:S(2)}, u32[]{:S(2)}) async-start(bf16[64,10,2048]{2,1,0:T(8,128)(2,1)} %reshape.78), calls=%async_computation.1 | async-start | bytes 8388608 | tf_op jit(solution)/shard_map/all_to_all | solution.py:50
  855.3 5.3 copy-start.2
where the time goes:
time: 866 us; the launch traced here: 865 us
  blocking collectives  412 us (48%)
  waiting for transfers between devices  379 us (44%)
  local copies, waits for them, and re-layouts  42.3 us (5%)
  matrix products  20.1 us (2%)
  starting transfers between devices  8.77 us (1%)
    all_to_all x1, blocking collectives, on_device(): lax.all_to_all(outgoing, 'ep', split_axis=0, concat_axis=0, tiled=True)  412 us
    all_to_all x1, waiting for transfers between devices, on_device(): lax.all_to_all(expert_rows.reshape(devices_ep, capacity, model_width), 'e...  379 us
  transfers between devices with their start and end apart: 1, of which 1 were waited for; matrix products, arithmetic and copies ran while one was open for 0% of the time, Pallas kernels for 0%

commit v1 on v0

--- a/solution.py
+++ b/solution.py
@@ -41,14 +41,14 @@
         jnp.full((devices_ep * capacity,), tok_rows, jnp.int32).at[slot_index].set(pair_token)
     )
     padded = jnp.concatenate([normed, jnp.zeros((1, model_width), jnp.bfloat16)], axis=0)
-    outgoing = padded[slot_token].reshape(devices_ep, capacity, model_width)
+    outgoing = padded[slot_token].reshape(devices_ep, 160, 128)
     arrived = lax.all_to_all(outgoing, "ep", split_axis=0, concat_axis=0, tiled=True)
     flat_rows = arrived.reshape(devices_ep * capacity, model_width)
     expert_rows = swiglu_rows(flat_rows, expert_gate[0], expert_up[0], expert_down[0]).astype(
         jnp.bfloat16
     )
     returned = lax.all_to_all(
-        expert_rows.reshape(devices_ep, capacity, model_width),
+        expert_rows.reshape(devices_ep, 160, 128),
         "ep",
         split_axis=0,
         concat_axis=0,

time: 866 us -> 595 us (0.69)
  blocking collectives: 412 us -> 278 us
  waiting for transfers between devices: 379 us -> 245 us
    all_to_all x1, waiting for transfers between devices: 379 us -> 245 us  [on_device(): lax.all_to_all(expert_rows.reshape(devices_ep, 160, 128), 'ep', split_axi...]
    all_to_all x1, blocking collectives: 412 us -> 278 us  [on_device(): lax.all_to_all(outgoing, 'ep', split_axis=0, concat_axis=0, tiled=True)]
where the time goes in v1:
time: 595 us; the launch traced here: 594 us
  blocking collectives  278 us (47%)
  waiting for transfers between devices  245 us (41%)
  local copies, waits for them, and re-layouts  41.4 us (7%)
  matrix products  20.1 us (3%)
  starting transfers between devices  7.65 us (1%)
    all_to_all x1, blocking collectives, on_device(): lax.all_to_all(outgoing, 'ep', split_axis=0, concat_axis=0, tiled=True)  278 us
    all_to_all x1, waiting for transfers between devices, on_device(): lax.all_to_all(expert_rows.reshape(devices_ep, 160, 128), 'ep', split_axi...  245 us
  transfers between devices with their start and end apart: 1, of which 1 were waited for; matrix products, arithmetic and copies ran while one was open for 0% of the time, Pallas kernels for 0%

profile of v1, /device:TPU:37, one launch (start us, length us, event | category | flops | bytes accessed | tf_op | source)
XLA Modules:
  0.0 594.4 jit_solution(1161895078150590862)
XLA Ops:
  0.0 0.0 copy-start
  0.0 0.0 copy-start.1
  0.0 0.0 copy-start.4
  0.0 1.0 copy.12
  1.0 0.1 eq.29
  1.1 0.1 eq.25
  1.3 0.7 broadcast_multiply_fusion
  2.0 1.2 reduce-window.6
  3.2 0.2 slice_reduce_fusion
  3.5 0.1 fusion.23
  3.6 0.1 copy.11
  3.7 0.1 mul.59
  3.9 2.4 scatter_custom_fusion
  6.4 0.0 copy-done.1
  6.4 0.3 fusion.1
  6.7 0.0 copy-done.4
  6.7 0.3 fusion.3
  7.0 0.1 concatenate.3
  7.1 4.1 gather_fusion
  11.2 5.3 reshape.76
  16.5 277.8 %all_to_all.10 = bf16[64,160,128]{2,1,0:T(8,128)(2,1)} all-to-all(bf16[64,160,128]{2,1,0:T(8,128)(2,1)} %reshape.76), channel_id=1, replica_groups=mesh['grp'=4,'ep'=64] {'ep'}, dimensions={0} | all-to-all | bytes 5242880 | tf_op jit(solution)/shard_map/all_to_all | solution.py:45
  294.3 0.0 copy-start.6
  294.3 5.3 reshape.77
  299.6 0.0 copy-done.6
  299.6 3.4 fusion.9
  303.0 0.0 copy-done
  303.0 6.5 %convolution_convert_fusion = bf16[640,2048]{1,0:T(8,128)(2,1)} fusion(bf16[640,2048]{1,0:T(8,128)(2,1)} %reshape.77, bf16[1,256,2048]{2,1,0:T(8,128)(2,1)S(1)} %copy-done, bf16[1,2048,256]{2,1,0:T(8,128)(2,1)} %param.15, f32[640,256]{1,0:T(8,128)} %fusion.9), kind=kOutput, calls=%fused_computation.3 | convolution fusion | flops 1344471040 | bytes 7995392 | tf_op jit(solution)/shard_map/dot_general | solution.py:11
  309.5 5.2 reshape.78
  314.8 0.0 copy-start.5
  314.8 0.0 copy-start.3
  314.8 7.6 %all-to-all-start.1 = ((bf16[64,160,128]{2,1,0:T(8,128)(2,1)}), bf16[64,160,128]{2,1,0:T(8,128)(2,1)}, u32[]{:S(2)}, u32[]{:S(2)}) async-start(bf16[64,160,128]{2,1,0:T(8,128)(2,1)} %reshape.78), calls=%async_computation.1 | async-start | bytes 5242880 | tf_op jit(solution)/shard_map/all_to_all | solution.py:50
  322.4 0.0 copy-done.5
  322.5 0.2 copy.15
  322.6 0.0 copy-done.3
  322.7 0.4 fusion.34
  323.1 244.7 %all-to-all-done.1 = bf16[64,160,128]{2,1,0:T(8,128)(2,1)} async-done(((bf16[64,160,128]{2,1,0:T(8,128)(2,1)}), bf16[64,160,128]{2,1,0:T(8,128)(2,1)}, u32[]{:S(2)}, u32[]{:S(2)}) %all-to-all-start.1) | async-done | bytes 2621472 | tf_op jit(solution)/shard_map/all_to_all | solution.py:50
  567.8 5.2 reshape.79
  573.0 7.4 %gather_fusion.1 = bf16[512,2048]{1,0:T(8,128)(2,1)} fusion(bf16[640,2048]{1,0:T(8,128)(2,1)} %reshape.79, s32[1024]{0:T(1024)S(1)} %pad_clamp_fusion), kind=kCustom, calls=%fused_computation.1 | custom fusion | bytes 4196352 | tf_op jit(solution)/shard_map/gather | solution.py:57
  580.3 4.4 reshape.80
  584.7 0.0 copy-start.2
  584.7 5.3 fusion.33
  590.1 0.0 copy-done.2
  590.1 4.4 fusion
  (10 shorter events, 0.1 us)
Async XLA Ops:
  0.0 303.0 %copy-start = (bf16[1,256,2048]{2,1,0:T(8,128)(2,1)S(1)}, bf16[1,256,2048]{2,1,0:T(8,128)(2,1)}, u32[]{:S(2)}) copy-start(bf16[1,256,2048]{2,1,0:T(8,128)(2,1)} %param.16) | copy-start | bytes 3145732
  0.0 6.4 %copy-start.1 = (bf16[256,2048]{1,0:T(8,128)(2,1)S(1)}, bf16[256,2048]{1,0:T(8,128)(2,1)}, u32[]{:S(2)}) copy-start(bf16[256,2048]{1,0:T(8,128)(2,1)} %param.10) | copy-start | bytes 3145732
  0.0 6.7 %copy-start.4 = (f32[2048]{0:T(1024)S(1)}, f32[2048]{0:T(1024)}, u32[]{:S(2)}) copy-start(f32[2048]{0:T(1024)} %param.11) | copy-start | bytes 24580
  294.3 5.3 copy-start.6
  314.8 7.7 %copy-start.5 = (f32[256,2]{0,1:T(2,128)S(1)}, f32[256,2]{0,1:T(2,128)}, u32[]{:S(2)}) copy-start(f32[256,2]{0,1:T(2,128)} %param.13) | copy-start | bytes 6148
  314.8 7.9 %copy-start.3 = (bf16[2048,256]{1,0:T(8,128)(2,1)S(1)}, bf16[2048,256]{1,0:T(8,128)(2,1)}, u32[]{:S(2)}) copy-start(bf16[2048,256]{1,0:T(8,128)(2,1)} %param.17) | copy-start | bytes 3145732
  314.8 253.0 %all-to-all-start.1 = ((bf16[64,160,128]{2,1,0:T(8,128)(2,1)}), bf16[64,160,128]{2,1,0:T(8,128)(2,1)}, u32[]{:S(2)}, u32[]{:S(2)}) async-start(bf16[64,160,128]{2,1,0:T(8,128)(2,1)} %reshape.78), calls=%async_computation.1 | async-start | bytes 5242880 | tf_op jit(solution)/shard_map/all_to_all | solution.py:50
  584.7 5.3 copy-start.2
